TPU v7x, 32 devices: a whole 2x2x4 slice. The times are simulated.
32 devices in a mesh: sp: 8 (over z, x), tp: 4 (over y, core).
Axes of the slice: x: 2, y: 2, z: 4, core: 2. Of those that a mesh axis runs over, the one named last changes fastest.
Arguments:
- tokens: bfloat16 [4096, 4096], P('sp', 'tp'), may hold values from -8 to 8
- w_key: bfloat16 [4096, 2048], P(None, 'tp'), may hold values from -0.09375 to 0.09375
- w_value: bfloat16 [4096, 2048], P(None, 'tp'), may hold values from -0.09375 to 0.09375
- w_beta: bfloat16 [4096, 16], replicated, may hold values from -0.09375 to 0.09375
- w_decay: bfloat16 [4096, 16], replicated, may hold values from -0.09375 to 0.09375
- beta_bias: float32 [16], replicated, may hold values from -6 to -4
- decay_rate: float32 [16], replicated, as said below
- forgetting_increment: float32 [16, 4096], P('tp', 'sp')
- new_query: bfloat16 [16, 128], P('tp', 'sp'), may hold values from -6 to 6
- read_gain: bfloat16 [128], replicated, may hold values from 0.099609375 to 1.8984375
Outputs:
- state_cache: bfloat16 [16, 128, 128], P('tp', 'sp')
- first_read: float32 [16, 128], P('tp')
Inputs may be any that keep to these rules, and one draw needn't show every extreme that they name: `decay_rate`: positive.
All inputs are finite; a program needn't handle non-finite values.
Results may differ from a plain program's by a relative error of at most 0.0075.
Values may be sent and summed in bfloat16 or wider, within the bound.
A program may use at most 64 MiB of HBM per device.

v0:
```python
import functools

import jax
import jax.numpy as jnp
from jax import lax
from jax.experimental import pallas as pl
from jax.experimental.pallas import tpu as pltpu
from jax.sharding import PartitionSpec as P

DK = 128
DV = 128
CHUNK = 128
LANES = 128
SUB = 8
norm_eps = 1e-06
MESH = pl.DeviceIdType.MESH
F32 = jnp.float32
BF16 = jnp.bfloat16


def mm(left, right):
    return jnp.dot(left.astype(BF16), right.astype(BF16), preferred_element_type=F32)


def mm_nt(left, right):
    return lax.dot_general(
        left.astype(BF16), right.astype(BF16), (((1,), (1,)), ((), ())), preferred_element_type=F32
    )


def log2(value):
    return value.bit_length() - 1


def tail_pieces(features):
    return 4 if features % 1024 == 0 else 1


def body(
    n_sp,
    n_tp,
    x_hbm,
    wk_hbm,
    wv_hbm,
    wb_hbm,
    wd_hbm,
    bias_ref,
    rate_ref,
    finc_ref,
    q_ref,
    gain_ref,
    state_out,
    read_out,
    wk,
    wv,
    wb,
    wd,
    wg,
    x_ref,
    finc8,
    q_own,
    xg,
    acck,
    accv,
    accg,
    maps,
    gams,
    sendbuf,
    recvbuf,
    gsend,
    grecv,
    qslots,
    fstate,
    srecv,
    fread,
    rrecv,
    wsem,
    own_send,
    peer_send,
    fwd_send,
    tok_recv,
    q_send,
    q_recv,
    map_send,
    map_recv,
    g_send,
    g_recv,
    s_send,
    s_recv,
    r_send,
    r_recv,
):
    sp = lax.axis_index("sp")
    tp = lax.axis_index("tp")
    tokens_here, features = x_ref.shape
    heads = wk.shape[1] // DK
    chunks = tokens_here // CHUNK
    last = chunks - 1
    pieces = tail_pieces(features)
    wide = features // pieces
    parts = last + pieces
    n_y = n_tp // 2
    y = tp // 2
    core = tp % 2
    sibling = tp + 1 - 2 * core
    levels = log2(n_sp)
    rows_out = DK // n_sp

    load_x = pltpu.make_async_copy(x_hbm, x_ref, wsem.at[4])
    load_x.start()
    loads = [
        pltpu.make_async_copy(wk_hbm, wk, wsem.at[0]),
        pltpu.make_async_copy(wv_hbm, wv, wsem.at[1]),
        pltpu.make_async_copy(wb_hbm, wb, wsem.at[2]),
        pltpu.make_async_copy(wd_hbm, wd, wsem.at[3]),
    ]
    for load in (loads[2], loads[3], loads[0], loads[1]):
        load.start()

    barrier = pltpu.get_barrier_semaphore()
    pl.semaphore_signal(barrier, inc=1, device_id={"tp": sibling}, device_id_type=MESH)
    for step in range(1, n_y):
        peer = ((y + step) % n_y) * 2 + core
        pl.semaphore_signal(barrier, inc=1, device_id={"tp": peer}, device_id_type=MESH)
    masks = sorted(set(range(1, heads)) | {1 << level for level in range(levels)})

    def flip(mask):
        found = sp
        for place in range(levels):
            if (mask >> place) % 2:
                found = found + (1 - 2 * ((sp // (1 << place)) % 2)) * (1 << place)
        return found

    for mask in masks:
        pl.semaphore_signal(barrier, inc=1, device_id={"sp": flip(mask)}, device_id_type=MESH)

    def part_of(k):
        if isinstance(k, int) and k >= last:
            return pl.ds(last * CHUNK, CHUNK), pl.ds((k - last) * wide, wide)
        start = k * CHUNK if isinstance(k, int) else pl.multiple_of(k * CHUNK, CHUNK)
        return pl.ds(start, CHUNK), pl.ds(0, features)

    def copy_own(k):
        rows, cols = part_of(k)
        return pltpu.make_async_remote_copy(
            src_ref=x_ref.at[rows, cols],
            dst_ref=xg.at[tp, rows, cols],
            send_sem=own_send.at[k],
            recv_sem=tok_recv.at[tp, k],
            device_id={"tp": sibling},
            device_id_type=MESH,
        )

    def copy_peer(step, k):
        rows, cols = part_of(k)
        peer = ((y + step) % n_y) * 2 + core
        return pltpu.make_async_remote_copy(
            src_ref=x_ref.at[rows, cols],
            dst_ref=xg.at[tp, rows, cols],
            send_sem=peer_send.at[step, k],
            recv_sem=tok_recv.at[tp, k],
            device_id={"tp": peer},
            device_id_type=MESH,
        )

    def copy_forward(step, k):
        rows, cols = part_of(k)
        source = ((y + n_y - step) % n_y) * 2 + core
        return pltpu.make_async_remote_copy(
            src_ref=xg.at[source, rows, cols],
            dst_ref=xg.at[source, rows, cols],
            send_sem=fwd_send.at[step, k],
            recv_sem=tok_recv.at[source, k],
            device_id={"tp": sibling},
            device_id_type=MESH,
        )

    def arrived(source, k):
        rows, cols = part_of(k)
        pltpu.make_async_remote_copy(
            src_ref=xg.at[source, rows, cols],
            dst_ref=xg.at[source, rows, cols],
            send_sem=own_send.at[k],
            recv_sem=tok_recv.at[source, k],
            device_id={"tp": sibling},
            device_id_type=MESH,
        ).wait_recv()

    pl.semaphore_wait(barrier, n_y + len(masks))
    load_x.wait()
    for k in range(parts):
        for step in range(1, n_y):
            copy_peer(step, k).start()
        copy_own(k).start()

    rows_q = lax.broadcasted_iota(jnp.int32, (rows_out, LANES), 0)
    lanes_q = lax.broadcasted_iota(jnp.int32, (rows_out, LANES), 1)
    place_q = jnp.where(lanes_q == rows_q + sp * rows_out, 1.0, 0.0)
    q_own[...] = jnp.zeros_like(q_own)
    q_own[0:heads, :] = mm(q_ref[...], place_q)
    qslots[sp] = q_own[...]

    lead = heads // 2
    bit0 = sp % 2

    def actual(i):
        return (i + (1 - bit0) * lead) % heads if heads > 1 else i

    finc8[...] = jnp.zeros_like(finc8)
    for i in range(heads):
        finc8[i : i + 1, :] = finc_ref[pl.ds(actual(i), 1), :]

    total_heads = wb.shape[0]
    row_id = lax.broadcasted_iota(jnp.int32, (LANES, total_heads), 0)
    col_id = lax.broadcasted_iota(jnp.int32, (LANES, total_heads), 1)
    first_head = tp * heads
    shift = (1 - bit0) * lead
    own_head = first_head + (row_id % SUB + shift) % heads
    own = (row_id % SUB < heads) & (col_id == own_head)
    pick_b = jnp.where(own & (row_id < SUB), 1.0, 0.0)
    pick_d = jnp.where(own & (row_id >= SUB) & (row_id < 2 * SUB), 1.0, 0.0)
    loads[2].wait()
    loads[3].wait()
    depth = wg.shape[0]
    piece = 512

    def pick(step, carry):
        rows = pl.ds(pl.multiple_of(step * piece, piece), piece)
        both = mm(pick_b, wb[:, rows]) + mm(pick_d, wd[:, rows])
        wg[rows, :] = jnp.transpose(both).astype(BF16)
        return carry

    lax.fori_loop(0, depth // piece, pick, 0)
    loads[0].wait()
    loads[1].wait()

    def project(x, source, rows, first=False, start=0, size=features):
        deep = pl.ds(pl.multiple_of(source * features + start, size), size)
        for acc, weights in ((acck, wk), (accv, wv), (accg, wg)):
            part = jnp.dot(x, weights[deep, :], preferred_element_type=F32)
            acc[rows, :] = part if first else acc[rows, :] + part

    half_rows = 256 if tokens_here % 256 == 0 else CHUNK

    def own_project(step, carry):
        rows = pl.ds(pl.multiple_of(step * half_rows, half_rows), half_rows)
        project(x_ref[rows, :], tp, rows, True)
        return carry

    lax.fori_loop(0, tokens_here // half_rows, own_project, 0)
    for k in range(parts):
        arrived(sibling, k)

    def sibling_project(step, carry):
        rows = pl.ds(pl.multiple_of(step * half_rows, half_rows), half_rows)
        project(xg[sibling, rows, :], sibling, rows)
        return carry

    lax.fori_loop(0, tokens_here // half_rows, sibling_project, 0)

    row8 = lax.broadcasted_iota(jnp.int32, (SUB, total_heads), 0)
    lane8 = lax.broadcasted_iota(jnp.int32, (SUB, total_heads), 1)
    mine = (lane8 == first_head + (row8 + shift) % heads) & (row8 < heads)
    bias_col = jnp.sum(jnp.where(mine, bias_ref[...], 0.0), axis=1, keepdims=True)
    rate_col = jnp.sum(jnp.where(mine, rate_ref[...], 0.0), axis=1, keepdims=True)

    maps[...] = jnp.zeros_like(maps)
    gams[...] = jnp.ones_like(gams)

    def near(step):
        return ((y + n_y - step) % n_y) * 2 + core

    def far(step):
        return ((y + n_y - step) % n_y) * 2 + 1 - core

    def gate_terms(rows):
        ri = lax.broadcasted_iota(jnp.int32, (CHUNK, CHUNK), 0)
        ci = lax.broadcasted_iota(jnp.int32, (CHUNK, CHUNK), 1)
        strict = ri > ci
        upper = jnp.where(ri <= ci, 1.0, 0.0)
        gates = jnp.transpose(accg[rows, :])
        beta = jax.nn.sigmoid(gates[0:SUB, :] + bias_col)
        raw = gates[SUB : 2 * SUB, :]
        softplus = jnp.maximum(raw, 0.0) + jnp.log1p(jnp.exp(-jnp.abs(raw)))
        logd = -rate_col * softplus + finc8[:, rows]
        cum = jnp.dot(logd, upper, precision=lax.Precision.HIGHEST, preferred_element_type=F32)
        total = jnp.sum(logd, axis=1, keepdims=True)
        columns = jnp.transpose(
            jnp.concatenate(
                [
                    beta,
                    cum,
                    jnp.exp(cum),
                    jnp.exp(total - cum),
                    jnp.zeros((LANES - 4 * SUB, LANES), F32),
                ],
                axis=0,
            )
        )
        return strict, cum, columns, jnp.exp(total)

    def advance(rows, terms, chosen):
        strict, cum, columns, keep = terms
        rights, powers, remains = [], [], []
        for h in chosen:
            cols = pl.ds(pl.multiple_of(actual(h) * DK, DK), DK)
            key = acck[rows, cols].astype(BF16).astype(F32)
            key = key * lax.rsqrt(jnp.sum(key * key, axis=-1, keepdims=True) + norm_eps)
            value = accv[rows, cols].astype(BF16).astype(F32)
            b_col = columns[:, h : h + 1]
            c_col = columns[:, SUB + h : SUB + h + 1]
            e_col = columns[:, 2 * SUB + h : 2 * SUB + h + 1]
            r_col = columns[:, 3 * SUB + h : 3 * SUB + h + 1]
            key_beta = key * b_col
            decay = jnp.exp(jnp.where(strict, c_col - cum[h : h + 1, :], 0.0))
            powers.append(jnp.where(strict, mm_nt(key_beta, key) * decay, 0.0))
            rights.append(jnp.concatenate([value * b_col, key_beta * e_col], axis=1))
            remains.append(jnp.transpose(key * r_col))
        solved = [right - mm(power, right) for power, right in zip(powers, rights)]
        covered = 2
        while covered < CHUNK:
            powers = [mm(power, power) for power in powers]
            solved = [known + mm(power, known) for power, known in zip(powers, solved)]
            covered *= 2
        fresh = []
        for h, known in zip(chosen, solved):
            gamma = gams[h, 0:1, 0:1]
            erase = known[:, DV:]
            direct = jnp.concatenate([known[:, :DV], -gamma * erase], axis=1)
            fresh.append(direct - mm(erase, maps[h]))
        for h, remain, new in zip(chosen, remains, fresh):
            maps[h] = keep[h : h + 1, 0:1] * maps[h] + mm(remain, new)
            gams[h] = keep[h : h + 1, 0:1] * gams[h]

    def chunk_step(c, carry):
        rows = pl.ds(pl.multiple_of(c * CHUNK, CHUNK), CHUNK)
        for step in range(1, n_y):
            arrived(near(step), c)
            copy_forward(step, c).start()
        for step in range(1, n_y):
            project(xg[near(step), rows, :], near(step), rows)
        for step in range(1, n_y):
            arrived(far(step), c)
            project(xg[far(step), rows, :], far(step), rows)
        advance(rows, gate_terms(rows), range(heads))
        return carry

    lax.fori_loop(0, last, chunk_step, 0)

    def far_part(k):
        rows, cols = part_of(k)
        for step in range(1, n_y):
            arrived(far(step), k)
            project(xg[far(step), rows, cols], far(step), rows, False, (k - last) * wide, wide)

    end_rows = pl.ds(last * CHUNK, CHUNK)
    for k in range(last, parts):
        rows, cols = part_of(k)
        for step in range(1, n_y):
            arrived(near(step), k)
            copy_forward(step, k).start()
        for step in range(1, n_y):
            project(xg[near(step), rows, cols], near(step), rows, False, (k - last) * wide, wide)
        if k > last:
            far_part(k - 1)
    far_part(parts - 1)
    end_terms = gate_terms(end_rows)

    count = heads
    offset = 0
    held = 0
    for level in range(levels):
        bit = (sp // (1 << level)) % 2
        partner = flip(1 << level)
        split = count > 1
        half = count // 2 if split else count
        if level == 0:
            send_at, keep_at = 0, heads - half
            advance(end_rows, end_terms, range(half))
        else:
            keep_at = held + (bit * half if split else 0)
            send_at = held + ((1 - bit) * half if split else 0)
        rows = pl.ds(offset, half)
        known_q = pl.ds(sp - sp % (1 << level), 1 << level)
        move_q = pltpu.make_async_remote_copy(
            src_ref=qslots.at[known_q],
            dst_ref=qslots.at[known_q],
            send_sem=q_send.at[level],
            recv_sem=q_recv.at[level],
            device_id={"sp": partner},
            device_id_type=MESH,
        )
        for i in range(half):
            sendbuf[offset + i] = maps[send_at + i].astype(BF16)
            gsend[offset + i] = gams[send_at + i]
        move = pltpu.make_async_remote_copy(
            src_ref=sendbuf.at[rows],
            dst_ref=recvbuf.at[rows],
            send_sem=map_send.at[level],
            recv_sem=map_recv.at[level],
            device_id={"sp": partner},
            device_id_type=MESH,
        )
        move_g = pltpu.make_async_remote_copy(
            src_ref=gsend.at[rows],
            dst_ref=grecv.at[rows],
            send_sem=g_send.at[level],
            recv_sem=g_recv.at[level],
            device_id={"sp": partner},
            device_id_type=MESH,
        )
        move.start()
        move_g.start()
        move_q.start()
        if level == 0 and split:
            advance(end_rows, end_terms, range(half, heads))
        move.wait()
        move_g.wait()
        move_q.wait()
        later = bit == 1
        for i in range(half):
            own = maps[keep_at + i]
            if not split:
                own = own.astype(BF16).astype(F32)
            own_g = gams[keep_at + i]
            got = recvbuf[offset + i].astype(F32)
            got_g = grecv[offset + i]
            left = jnp.where(later, own, got)
            left_g = jnp.where(later, own_g, got_g)
            right = jnp.where(later, got, own)
            right_g = jnp.where(later, got_g, own_g)
            tail = left[:, DV:]
            added = jnp.concatenate([left[:, :DV], right_g[0:1, 0:1] * tail], axis=1)
            maps[keep_at + i] = left_g[0:1, 0:1] * right + mm(tail, right) + added
            gams[keep_at + i] = left_g * right_g
        offset += half
        count = half
        held = keep_at

    my_head = bit0 * lead + held - lead if heads > 1 else 0
    final = maps[held][:, :DV]
    for j in range(n_sp):
        fstate[j] = final[j * rows_out : (j + 1) * rows_out, :].astype(BF16)

    def head_of(index):
        found = 0
        for place in range(log2(heads)):
            found = found * 2 + (index // (1 << place)) % 2
        return found

    def copy_state(step):
        target = flip(step)
        return pltpu.make_async_remote_copy(
            src_ref=fstate.at[target],
            dst_ref=srecv.at[my_head],
            send_sem=s_send.at[step],
            recv_sem=s_recv.at[my_head],
            device_id={"sp": target},
            device_id_type=MESH,
        )

    for step in range(1, heads):
        copy_state(step).start()
    srecv[my_head] = fstate[sp]

    query = jnp.sum(qslots[...], axis=0)
    reads = mm(query, final)
    row_head = lax.broadcasted_iota(jnp.int32, (SUB, DV), 0)
    raw_read = jnp.sum(jnp.where(row_head == my_head, reads, 0.0), axis=0, keepdims=True)
    read = (
        raw_read
        * lax.rsqrt(jnp.mean(raw_read * raw_read, axis=-1, keepdims=True) + norm_eps)
        * gain_ref[...].astype(F32)
    )
    fread[...] = jnp.broadcast_to(read, fread.shape)

    def copy_read(step):
        target = flip(step)
        return pltpu.make_async_remote_copy(
            src_ref=fread,
            dst_ref=rrecv.at[my_head],
            send_sem=r_send.at[step],
            recv_sem=r_recv.at[my_head],
            device_id={"sp": target},
            device_id_type=MESH,
        )

    for step in range(1, heads):
        copy_read(step).start()
    rrecv[my_head] = fread[...]

    for step in range(1, heads):
        source = flip(step)
        head = head_of(source)
        pltpu.make_async_remote_copy(
            src_ref=fstate.at[source],
            dst_ref=srecv.at[head],
            send_sem=s_send.at[step],
            recv_sem=s_recv.at[head],
            device_id={"sp": source},
            device_id_type=MESH,
        ).wait_recv()
        pltpu.make_async_remote_copy(
            src_ref=fread,
            dst_ref=rrecv.at[head],
            send_sem=r_send.at[step],
            recv_sem=r_recv.at[head],
            device_id={"sp": source},
            device_id_type=MESH,
        ).wait_recv()
    for h in range(heads):
        state_out[h] = srecv[h]
        read_out[h : h + 1, :] = rrecv[h, 0:1, :]

    for k in range(parts):
        copy_own(k).wait_send()
        for step in range(1, n_y):
            copy_peer(step, k).wait_send()
            copy_forward(step, k).wait_send()
    for step in range(1, heads):
        copy_state(step).wait_send()
        copy_read(step).wait_send()


def hand_over(state_ref, read_ref, state_out, read_out):
    state_out[...] = state_ref[...]
    read_out[...] = read_ref[...]


def per_device(
    n_sp,
    n_tp,
    tokens,
    w_key,
    w_value,
    w_beta,
    w_decay,
    beta_bias,
    decay_rate,
    forgetting_increment,
    new_query,
    read_gain,
):
    tokens_here, features = tokens.shape
    depth, width = w_key.shape
    heads = width // DK
    parts = tokens_here // CHUNK - 1 + tail_pieces(features)
    rows_out = DK // n_sp
    n_y = n_tp // 2
    levels = log2(n_sp)
    slots = 0
    count = heads
    for _ in range(levels):
        count = max(count // 2, 1)
        slots += count
    vmem = pl.BlockSpec(memory_space=pltpu.VMEM)
    hbm = pl.BlockSpec(memory_space=pl.ANY)
    dma = pltpu.SemaphoreType.DMA
    state, read = pl.pallas_call(
        functools.partial(body, n_sp, n_tp),
        name="delta_state",
        out_shape=(
            jax.ShapeDtypeStruct((heads, rows_out, DV), BF16),
            jax.ShapeDtypeStruct((heads, DV), F32),
        ),
        in_specs=[hbm, hbm, hbm, hbm, hbm, vmem, vmem, vmem, vmem, vmem],
        out_specs=(vmem, vmem),
        scratch_shapes=[
            pltpu.VMEM((depth, width), BF16),
            pltpu.VMEM((depth, width), BF16),
            pltpu.VMEM(w_beta.shape[::-1], BF16),
            pltpu.VMEM(w_decay.shape[::-1], BF16),
            pltpu.VMEM((depth, LANES), BF16),
            pltpu.VMEM((tokens_here, features), BF16),
            pltpu.VMEM((SUB, tokens_here), F32),
            pltpu.VMEM((SUB, DK), F32),
            pltpu.VMEM((n_tp, tokens_here, features), BF16),
            pltpu.VMEM((tokens_here, width), F32),
            pltpu.VMEM((tokens_here, width), F32),
            pltpu.VMEM((tokens_here, LANES), F32),
            pltpu.VMEM((heads, DK, DV + DK), F32),
            pltpu.VMEM((heads, SUB, LANES), F32),
            pltpu.VMEM((slots, DK, DV + DK), BF16),
            pltpu.VMEM((slots, DK, DV + DK), BF16),
            pltpu.VMEM((slots, SUB, LANES), F32),
            pltpu.VMEM((slots, SUB, LANES), F32),
            pltpu.VMEM((n_sp, SUB, DK), F32),
            pltpu.VMEM((n_sp, rows_out, DV), BF16),
            pltpu.VMEM((heads, rows_out, DV), BF16),
            pltpu.VMEM((SUB, DV), F32),
            pltpu.VMEM((heads, SUB, DV), F32),
            dma((5,)),
            dma((parts,)),
            dma((n_y, parts)),
            dma((n_y, parts)),
            dma((n_tp, parts)),
            dma((levels,)),
            dma((levels,)),
            dma((levels,)),
            dma((levels,)),
            dma((levels,)),
            dma((levels,)),
            dma((heads,)),
            dma((heads,)),
            dma((heads,)),
            dma((heads,)),
        ],
        compiler_params=pltpu.CompilerParams(
            collective_id=0, has_side_effects=True, vmem_limit_bytes=60 * 1024 * 1024
        ),
    )(
        tokens,
        w_key,
        w_value,
        w_beta.T,
        w_decay.T,
        beta_bias[None, :],
        decay_rate[None, :],
        forgetting_increment,
        new_query,
        read_gain[None, :],
    )
    return pl.pallas_call(
        hand_over,
        name="hand_over",
        out_shape=(
            jax.ShapeDtypeStruct(state.shape, state.dtype),
            jax.ShapeDtypeStruct(read.shape, read.dtype),
        ),
        in_specs=[vmem, vmem],
        out_specs=(vmem, vmem),
    )(state, read)


def solution(mesh):
    return jax.shard_map(
        functools.partial(per_device, mesh.shape["sp"], mesh.shape["tp"]),
        mesh=mesh,
        in_specs=(
            P("sp", "tp"),
            P(None, "tp"),
            P(None, "tp"),
            P(),
            P(),
            P(),
            P(),
            P("tp", "sp"),
            P("tp", "sp"),
            P(),
        ),
        out_specs=(P("tp", "sp", None), P("tp", None)),
        check_vma=False,
    )
```

profile of v0, /device:TPU:0, one launch (start us, length us, event | category | flops | bytes accessed | tf_op | source)
XLA Modules:
  0.0 55.8 jit_solution(9779823972673796272)
XLA Ops:
  0.6 53.8 %delta_state.1 = (bf16[4,16,128]{2,1,0:T(8,128)(2,1)}, f32[4,128]{1,0:T(4,128)}) custom-call(bf16[512,1024]{1,0:T(8,128)(2,1)} %x_hbm.1, bf16[4096,512]{1,0:T(8,128)(2,1)} %wk_hbm.1, bf16[4096,512]{1,0:T(8,128)(2,1)} %wv_hbm.1, bf16[16,4096]{1,0:T(8,128)(2,1)} %bitcast.5, bf16[16,4096]{1,0:T(8,128)(2,1)} %bitcast.6, f32[1,16]{1,0:T(1,128)} %bitcast.7, ...), custom_call_target="tpu_custom_call" | custom-call | tf_op jit(solution)/shard_map/delta_state/pallas_call | solution.py:559
  54.4 1.3 %hand_over.1 = (bf16[4,16,128]{2,1,0:T(8,128)(2,1)}, f32[4,128]{1,0:T(4,128)}) custom-call(bf16[4,16,128]{2,1,0:T(8,128)(2,1)} %get-tuple-element.4.state_ref, f32[4,128]{1,0:T(4,128)} %get-tuple-element.5.read_ref), custom_call_target="tpu_custom_call" | custom-call | tf_op jit(solution)/shard_map/hand_over/pallas_call | solution.py:623
where the time goes:
time: 56 us; the launch traced here: 55.8 us
  Pallas kernels  55.1 us (98%)
  between operations  0.64 us (1%)
    pallas_call x1, Pallas kernels, per_device(): pl.pallas_call(functools.partial(body, n_sp, n_tp), name='delta_state', o...  53.8 us
    pallas_call x1, Pallas kernels, per_device(): pl.pallas_call(hand_over, name='hand_over', out_shape=(jax.ShapeDtypeStru...  1.33 us

commit v1 on v0

v1 whole, which is shorter than its diff:
```python
import functools

import jax
import jax.numpy as jnp
from jax import lax
from jax.experimental import pallas as pl
from jax.experimental.pallas import tpu as pltpu
from jax.sharding import PartitionSpec as P

DK = 128
DV = 128
CHUNK = 128
LANES = 128
SUB = 8
norm_eps = 1e-06
MESH = pl.DeviceIdType.MESH
F32 = jnp.float32
BF16 = jnp.bfloat16


def mm(left, right):
    return jnp.dot(left.astype(BF16), right.astype(BF16), preferred_element_type=F32)


def mm_nt(left, right):
    return lax.dot_general(
        left.astype(BF16), right.astype(BF16), (((1,), (1,)), ((), ())), preferred_element_type=F32
    )


def log2(value):
    return value.bit_length() - 1


def near_rounds(n_sp):
    return 2 if n_sp == 8 else 0


def tree_shape(n_sp, heads):
    joins = log2(n_sp) - 2
    splits = min(joins, log2(heads))
    width_z = heads >> splits
    return joins, splits, width_z, 1 << (joins - splits)


def tail_pieces(features):
    return 4 if features % 1024 == 0 else 1


def body(
    n_sp,
    n_tp,
    x_hbm,
    wk_hbm,
    wv_hbm,
    wb_hbm,
    wd_hbm,
    bias_hbm,
    rate_hbm,
    finc_hbm,
    q_hbm,
    gain_hbm,
    state_out,
    read_out,
    wk,
    wv,
    wb,
    wd,
    bias_ref,
    rate_ref,
    finc_ref,
    q_ref,
    gain_ref,
    wg,
    x_ref,
    finc8,
    q_own,
    xg,
    acck,
    accv,
    accg,
    maps,
    gams,
    sendbuf,
    recvbuf,
    gsend,
    grecv,
    zsend,
    zrecv,
    gzsend,
    gzrecv,
    qslots,
    q_wide,
    fstate,
    final_ref,
    fread,
    rrecv,
    wsem,
    ready,
    own_recv,
    tok_recv,
    q_recv,
    map_recv,
    g_recv,
    z_recv,
    gz_recv,
    s_recv,
    r_recv,
):
    sp = lax.axis_index("sp")
    tp = lax.axis_index("tp")
    tokens_here, features = x_ref.shape
    heads = wk.shape[1] // DK
    chunks = tokens_here // CHUNK
    last = chunks - 1
    pieces = tail_pieces(features)
    wide = features // pieces
    parts = last + pieces
    n_y = n_tp // 2
    y = tp // 2
    core = tp % 2
    sibling = tp + 1 - 2 * core
    levels = log2(n_sp)
    rows_out = DK // n_sp
    joins, splits, width_z, copies = tree_shape(n_sp, heads)
    base = 1 << joins
    line_z = sp // base

    (map_send, z_send, s_send, r_send, tok_send, q_send, g_send, gz_send) = (
        wsem.at[pl.ds(place, 1)] for place in range(8)
    )
    barrier = pltpu.get_barrier_semaphore()

    def tell(semaphore, place):
        pl.semaphore_signal(semaphore, inc=1, device_id=place, device_id_type=MESH)

    def flip(mask):
        found = sp
        for place in range(levels):
            if (mask >> place) % 2:
                found = found + (1 - 2 * ((sp // (1 << place)) % 2)) * (1 << place)
        return found

    line = sp // 2
    lines = n_sp // 2

    def tell_near(semaphore):
        tell(semaphore, {"sp": flip(1)})

        @pl.when(line > 0)
        def _():
            tell(semaphore, {"sp": sp - 2})

        @pl.when(line < lines - 1)
        def _():
            tell(semaphore, {"sp": sp + 2})

    near_count = 1 + jnp.where(line > 0, 1, 0) + jnp.where(line < lines - 1, 1, 0)
    rounds = near_rounds(n_sp)

    for step in range(1, n_y):
        peer = ((y + step) % n_y) * 2 + core
        tell(barrier, {"tp": peer})
    tell(barrier, {"tp": sibling})
    if rounds:
        tell_near(barrier)
        greeted = n_y + near_count
    else:
        for mask in range(1, n_sp):
            tell(barrier, {"sp": flip(mask)})
        greeted = n_y + n_sp - 1

    load_x = pltpu.make_async_copy(x_hbm, x_ref, wsem.at[4])
    load_x.start()
    small = [
        pltpu.make_async_copy(source, target, wsem.at[5 + place])
        for place, (source, target) in enumerate(
            (
                (q_hbm, q_ref),
                (finc_hbm, finc_ref),
                (bias_hbm, bias_ref),
                (rate_hbm, rate_ref),
                (gain_hbm, gain_ref),
            )
        )
    ]
    loads = [
        pltpu.make_async_copy(wk_hbm, wk, wsem.at[0]),
        pltpu.make_async_copy(wv_hbm, wv, wsem.at[1]),
        pltpu.make_async_copy(wb_hbm, wb, wsem.at[2]),
        pltpu.make_async_copy(wd_hbm, wd, wsem.at[3]),
    ]
    for load in (*small, loads[2], loads[3], loads[0], loads[1]):
        load.start()

    def part_of(k):
        if isinstance(k, int) and k >= last:
            return pl.ds(last * CHUNK, CHUNK), pl.ds((k - last) * wide, wide)
        start = k * CHUNK if isinstance(k, int) else pl.multiple_of(k * CHUNK, CHUNK)
        return pl.ds(start, CHUNK), pl.ds(0, features)

    def copy_own(source):
        return pltpu.make_async_remote_copy(
            src_ref=x_ref,
            dst_ref=xg.at[source],
            send_sem=tok_send.at[0],
            recv_sem=own_recv.at[0],
            device_id={"tp": sibling},
            device_id_type=MESH,
        )

    def copy_peer(step, k):
        rows, cols = part_of(k)
        peer = ((y + step) % n_y) * 2 + core
        return pltpu.make_async_remote_copy(
            src_ref=x_ref.at[rows, cols],
            dst_ref=xg.at[tp, rows, cols],
            send_sem=tok_send.at[0],
            recv_sem=tok_recv.at[step - 1, k],
            device_id={"tp": peer},
            device_id_type=MESH,
        )

    def copy_forward(step, k):
        rows, cols = part_of(k)
        source = ((y + n_y - step) % n_y) * 2 + core
        return pltpu.make_async_remote_copy(
            src_ref=xg.at[source, rows, cols],
            dst_ref=xg.at[source, rows, cols],
            send_sem=tok_send.at[0],
            recv_sem=tok_recv.at[n_y - 2 + step, k],
            device_id={"tp": sibling},
            device_id_type=MESH,
        )

    def arrived(source, place, k):
        rows, cols = part_of(k)
        pltpu.make_async_remote_copy(
            src_ref=xg.at[source, rows, cols],
            dst_ref=xg.at[source, rows, cols],
            send_sem=tok_send.at[0],
            recv_sem=tok_recv.at[place, k],
            device_id={"tp": sibling},
            device_id_type=MESH,
        ).wait_recv()

    pl.semaphore_wait(barrier, greeted)
    load_x.wait()
    for k in range(parts):
        for step in range(1, n_y):
            copy_peer(step, k).start()
        if k == 0:
            copy_own(tp).start()
    if rounds:
        tell_near(ready.at[0])
    for load in small:
        load.wait()

    rows_q = lax.broadcasted_iota(jnp.int32, (rows_out, LANES), 0)
    lanes_q = lax.broadcasted_iota(jnp.int32, (rows_out, LANES), 1)
    place_q = jnp.where(lanes_q == rows_q + sp * rows_out, 1.0, 0.0)
    q_own[...] = jnp.zeros_like(q_own)
    q_own[0:heads, :] = mm(q_ref[...], place_q)

    lead = heads // 2
    bit0 = sp % 2
    turn = jnp.where(line_z < 2, 1, 0)

    def actual(i):
        if heads == 1:
            return i
        found = (i + (1 - bit0) * lead) % heads
        return found + turn * (1 - 2 * (found % 2)) if lead == 2 else found

    finc8[...] = jnp.zeros_like(finc8)
    for i in range(heads):
        finc8[i : i + 1, :] = finc_ref[pl.ds(actual(i), 1), :]

    total_heads = wb.shape[0]
    row_id = lax.broadcasted_iota(jnp.int32, (LANES, total_heads), 0)
    col_id = lax.broadcasted_iota(jnp.int32, (LANES, total_heads), 1)
    first_head = tp * heads
    own_head = first_head + actual(row_id % SUB)
    own = (row_id % SUB < heads) & (col_id == own_head)
    pick_b = jnp.where(own & (row_id < SUB), 1.0, 0.0)
    pick_d = jnp.where(own & (row_id >= SUB) & (row_id < 2 * SUB), 1.0, 0.0)
    loads[2].wait()
    loads[3].wait()
    depth = wg.shape[0]
    piece = 512

    def pick(step, carry):
        rows = pl.ds(pl.multiple_of(step * piece, piece), piece)
        both = mm(pick_b, wb[:, rows]) + mm(pick_d, wd[:, rows])
        wg[rows, :] = jnp.transpose(both).astype(BF16)
        return carry

    lax.fori_loop(0, depth // piece, pick, 0)
    loads[0].wait()
    loads[1].wait()

    def project(x, source, rows, first=False, start=0, size=features):
        deep = pl.ds(pl.multiple_of(source * features + start, size), size)
        for acc, weights in ((acck, wk), (accv, wv), (accg, wg)):
            part = jnp.dot(x, weights[deep, :], preferred_element_type=F32)
            acc[rows, :] = part if first else acc[rows, :] + part

    half_rows = 256 if tokens_here % 256 == 0 else CHUNK

    def own_project(step, carry):
        rows = pl.ds(pl.multiple_of(step * half_rows, half_rows), half_rows)
        project(x_ref[rows, :], tp, rows, True)
        return carry

    lax.fori_loop(0, tokens_here // half_rows, own_project, 0)
    copy_own(sibling).wait_recv()
    for step in range(1, rounds):
        pl.semaphore_wait(ready.at[step - 1], near_count)
        tell_near(ready.at[step])

    def sibling_project(step, carry):
        rows = pl.ds(pl.multiple_of(step * half_rows, half_rows), half_rows)
        project(xg[sibling, rows, :], sibling, rows)
        return carry

    lax.fori_loop(0, tokens_here // half_rows, sibling_project, 0)
    if rounds:
        pl.semaphore_wait(ready.at[rounds - 1], near_count)

    def owner_of(h, copy):
        return (1 + h % width_z) * base + h // width_z + (copy << splits)

    def copy_query(h, copy):
        owner = owner_of(h, copy)
        return pltpu.make_async_remote_copy(
            src_ref=q_own,
            dst_ref=qslots.at[sp],
            send_sem=q_send.at[0],
            recv_sem=q_recv.at[0],
            device_id={"sp": owner},
            device_id_type=MESH,
        )

    owners = [(h, copy) for h in range(heads) for copy in range(copies)]
    for h, copy in owners:

        @pl.when(sp != owner_of(h, copy))
        def _(h=h, copy=copy):
            copy_query(h, copy).start()

    row8 = lax.broadcasted_iota(jnp.int32, (SUB, total_heads), 0)
    lane8 = lax.broadcasted_iota(jnp.int32, (SUB, total_heads), 1)
    mine = (lane8 == first_head + actual(row8)) & (row8 < heads)
    bias_col = jnp.sum(jnp.where(mine, bias_ref[...], 0.0), axis=1, keepdims=True)
    rate_col = jnp.sum(jnp.where(mine, rate_ref[...], 0.0), axis=1, keepdims=True)

    maps[...] = jnp.zeros_like(maps)
    gams[...] = jnp.ones_like(gams)

    def near(step):
        return ((y + n_y - step) % n_y) * 2 + core

    def far(step):
        return ((y + n_y - step) % n_y) * 2 + 1 - core

    def gate_terms(rows):
        ri = lax.broadcasted_iota(jnp.int32, (CHUNK, CHUNK), 0)
        ci = lax.broadcasted_iota(jnp.int32, (CHUNK, CHUNK), 1)
        strict = ri > ci
        upper = jnp.where(ri <= ci, 1.0, 0.0).astype(BF16)
        gates = jnp.transpose(accg[rows, :])
        beta = jax.nn.sigmoid(gates[0:SUB, :] + bias_col)
        raw = gates[SUB : 2 * SUB, :]
        softplus = jnp.maximum(raw, 0.0) + jnp.log1p(jnp.exp(-jnp.abs(raw)))
        logd = -rate_col * softplus + finc8[:, rows]
        high = logd.astype(BF16).astype(F32)
        rest = logd - high
        middle = rest.astype(BF16).astype(F32)
        thirds = jnp.concatenate([high, middle, rest - middle], axis=0)
        sums = mm(thirds, upper)
        cum = sums[0:SUB] + sums[SUB : 2 * SUB] + sums[2 * SUB :]
        total = jnp.sum(logd, axis=1, keepdims=True)
        columns = jnp.transpose(
            jnp.concatenate(
                [
                    beta,
                    cum,
                    jnp.exp(cum),
                    jnp.exp(total - cum),
                    jnp.zeros((LANES - 4 * SUB, LANES), F32),
                ],
                axis=0,
            )
        )
        return strict, cum, columns, jnp.exp(total)

    def prepare(rows, chosen):
        found = []
        for h in chosen:
            cols = pl.ds(pl.multiple_of(actual(h) * DK, DK), DK)
            key = acck[rows, cols].astype(BF16).astype(F32)
            key = key * lax.rsqrt(jnp.sum(key * key, axis=-1, keepdims=True) + norm_eps)
            seen = mm(key, maps[h])
            erased = jnp.concatenate([seen[:, :DV], seen[:, DV:] + gams[h, 0:1, 0:1] * key], axis=1)
            found.append((key, mm_nt(key, key), erased))
        return found

    def advance(rows, terms, chosen, found=None, pause=None):
        strict, cum, columns, keep = terms
        found = prepare(rows, chosen) if found is None else found
        solved, powers, remains = [], [], []
        for h, (key, pairs, erased) in zip(chosen, found):
            cols = pl.ds(pl.multiple_of(actual(h) * DK, DK), DK)
            value = accv[rows, cols].astype(BF16).astype(F32)
            b_col = columns[:, h : h + 1]
            c_col = columns[:, SUB + h : SUB + h + 1]
            e_col = columns[:, 2 * SUB + h : 2 * SUB + h + 1]
            r_col = columns[:, 3 * SUB + h : 3 * SUB + h + 1]
            decay = jnp.exp(jnp.where(strict, c_col - cum[h : h + 1, :], 0.0))
            powers.append(jnp.where(strict, pairs * (b_col * decay), 0.0))
            gone = (b_col * e_col) * erased
            solved.append(jnp.concatenate([value * b_col - gone[:, :DV], -gone[:, DV:]], axis=1))
            remains.append(jnp.transpose(key * r_col))
        solved = [right - mm(power, right) for power, right in zip(powers, solved)]
        covered = 2
        while covered < CHUNK:
            powers = [mm(power, power) for power in powers]
            solved = [known + mm(power, known) for power, known in zip(powers, solved)]
            covered *= 2
            if covered == 16 and pause is not None:
                pause()
        for h, remain, new in zip(chosen, remains, solved):
            maps[h] = keep[h : h + 1, 0:1] * maps[h] + mm(remain, new)
            gams[h] = keep[h : h + 1, 0:1] * gams[h]

    def near_take(k):
        for step in range(1, n_y):
            arrived(near(step), step - 1, k)
            copy_forward(step, k).start()

    def far_take(k):
        for step in range(1, n_y):
            arrived(far(step), n_y - 2 + step, k)

    def take_in(side, rows):
        for step in range(1, n_y):
            project(xg[side(step), rows, :], side(step), rows)

    def chunk_step(c, carry):
        rows = pl.ds(pl.multiple_of(c * CHUNK, CHUNK), CHUNK)
        near_take(c)
        take_in(near, rows)
        far_take(c)
        take_in(far, rows)
        advance(rows, gate_terms(rows), range(heads))
        return carry

    end_rows = pl.ds(last * CHUNK, CHUNK)

    def end_project(side, place, number):
        cols = pl.ds(place * wide, number * wide)
        for step in range(1, n_y):
            project(
                xg[side(step), end_rows, cols],
                side(step),
                end_rows,
                False,
                place * wide,
                number * wide,
            )

    if pieces == 4 and last > 1:
        lax.fori_loop(0, last - 1, chunk_step, 0)
        before = last - 1
        rows = pl.ds(before * CHUNK, CHUNK)
        near_take(before)
        take_in(near, rows)

        @pl.when(core == 1)
        def _():
            near_take(last)
            near_take(last + 1)

        far_take(before)
        take_in(far, rows)

        @pl.when(core == 1)
        def _():
            near_take(last + 2)

        def pause():
            @pl.when(core == 1)
            def _():
                near_take(last + 3)

        advance(rows, gate_terms(rows), range(heads), pause=pause)

        @pl.when(core == 1)
        def _():
            end_project(near, 0, 4)
            far_take(last)
            far_take(last + 1)
            end_project(far, 0, 2)
            far_take(last + 2)
            end_project(far, 2, 1)
            far_take(last + 3)
            end_project(far, 3, 1)

        @pl.when(core == 0)
        def _():
            near_take(last)
            near_take(last + 1)
            end_project(near, 0, 2)
            near_take(last + 2)
            far_take(last)
            far_take(last + 1)
            end_project(far, 0, 2)
            end_project(near, 2, 1)
            far_take(last + 2)
            near_take(last + 3)
            far_take(last + 3)
            end_project(far, 2, 2)
            end_project(near, 3, 1)
    else:
        lax.fori_loop(0, last, chunk_step, 0)
        for place in range(pieces):
            near_take(last + place)
            end_project(near, place, 1)
        for place in range(pieces):
            far_take(last + place)
            end_project(far, place, 1)
    first_out = range(heads // 2 if heads > 1 else heads)
    end_found = prepare(end_rows, first_out)
    end_terms = gate_terms(end_rows)

    def copy_map(slot, part, partner):
        return pltpu.make_async_remote_copy(
            src_ref=sendbuf.at[slot, part],
            dst_ref=recvbuf.at[slot, part],
            send_sem=map_send.at[0],
            recv_sem=map_recv.at[slot, part],
            device_id={"sp": partner},
            device_id_type=MESH,
        )

    def copy_gamma(level, slot, number, partner):
        slots = pl.ds(slot, number)
        return pltpu.make_async_remote_copy(
            src_ref=gsend.at[slots],
            dst_ref=grecv.at[slots],
            send_sem=g_send.at[0],
            recv_sem=g_recv.at[level],
            device_id={"sp": partner},
            device_id_type=MESH,
        )

    def goal(j):
        return 1 + (turn + j) % 2 if width_z == 2 else 1

    def copy_up(j, part):
        return pltpu.make_async_remote_copy(
            src_ref=zsend.at[j, part],
            dst_ref=zrecv.at[line_z, part],
            send_sem=z_send.at[0],
            recv_sem=z_recv.at[line_z, part],
            device_id={"sp": sp % base + goal(j) * base},
            device_id_type=MESH,
        )

    def copy_up_gamma(j):
        return pltpu.make_async_remote_copy(
            src_ref=gzsend.at[j],
            dst_ref=gzrecv.at[line_z],
            send_sem=gz_send.at[0],
            recv_sem=gz_recv.at[line_z],
            device_id={"sp": sp % base + goal(j) * base},
            device_id_type=MESH,
        )

    count = heads
    offset = 0
    held = 0
    for level in range(joins):
        bit = (sp // (1 << level)) % 2
        later = bit == 1
        partner = flip(1 << level)
        split = count > 1
        half = count // 2 if split else count
        if level == 0:
            send_at, keep_at = 0, heads - half
        else:
            keep_at = held + (bit * half if split else 0)
            send_at = held + ((1 - bit) * half if split else 0)
        for j in range(half):
            if level == 0:
                gsend[j] = end_terms[3][j : j + 1, 0:1] * gams[j]
            else:
                gsend[offset + j] = gams[send_at + j]
        copy_gamma(level, offset, half, partner).start()
        if level == 0:
            advance(end_rows, end_terms, first_out, end_found)
        for j in range(half):
            slot = offset + j
            sendbuf[slot, 1] = maps[send_at + j, :, DV:].astype(BF16)
            copy_map(slot, 1, partner).start()
            sendbuf[slot, 0] = maps[send_at + j, :, :DV].astype(BF16)
            copy_map(slot, 0, partner).start()
        if level == 0 and split:
            advance(end_rows, end_terms, range(half, heads))
        top = level == joins - 1
        copy_gamma(level, offset, half, partner).wait_recv()
        if top:
            for j in range(half):
                gzsend[j] = gams[keep_at + j] * grecv[offset + j]

                @pl.when(jnp.logical_and(line_z != goal(j), line_z > 0))
                def _(j=j):
                    copy_up_gamma(j).start()

        for j in range(half):
            slot = offset + j
            own = maps[keep_at + j]
            if not split:
                own = own.astype(BF16).astype(F32)
            own_g = gams[keep_at + j]
            got_g = grecv[slot]
            left_g = jnp.where(later, own_g, got_g)[0:1, 0:1]
            right_g = jnp.where(later, got_g, own_g)[0:1, 0:1]
            gams[keep_at + j] = own_g * got_g
            copy_map(slot, 1, partner).wait_recv()
            got = recvbuf[slot, 1].astype(F32)
            left = jnp.where(later, own[:, DV:], got)
            right = jnp.where(later, got, own[:, DV:])
            joined = left_g * right + mm(left, right) + right_g * left
            maps[keep_at + j, :, DV:] = joined
            if top:
                zsend[j, 1] = joined.astype(BF16)

                @pl.when(jnp.logical_and(line_z != goal(j), line_z > 0))
                def _(j=j):
                    copy_up(j, 1).start()

            copy_map(slot, 0, partner).wait_recv()
            got = recvbuf[slot, 0].astype(F32)
            left_b = jnp.where(later, own[:, :DV], got)
            right_b = jnp.where(later, got, own[:, :DV])
            joined = left_g * right_b + mm(left, right_b) + left_b
            maps[keep_at + j, :, :DV] = joined
            if top:
                zsend[j, 0] = joined.astype(BF16)

                @pl.when(line_z != goal(j))
                def _(j=j):
                    copy_up(j, 0).start()

        offset += half
        count = half
        held = keep_at

    def copy_state(mask, h):
        target = flip(mask)
        return pltpu.make_async_remote_copy(
            src_ref=fstate.at[target],
            dst_ref=state_out.at[h],
            send_sem=s_send.at[0],
            recv_sem=s_recv.at[0],
            device_id={"sp": target},
            device_id_type=MESH,
        )

    def copy_read(mask, h):
        target = flip(mask)
        return pltpu.make_async_remote_copy(
            src_ref=fread,
            dst_ref=rrecv.at[h],
            send_sem=r_send.at[0],
            recv_sem=r_recv.at[0],
            device_id={"sp": target},
            device_id_type=MESH,
        )

    def settle(ref, sent, landed):
        return pltpu.make_async_remote_copy(
            src_ref=ref,
            dst_ref=ref,
            send_sem=sent.at[0],
            recv_sem=landed,
            device_id={"sp": sp},
            device_id_type=MESH,
        )

    free = [1 << place for place in range(levels) if place < splits or place >= joins]
    masks = [0]
    for place in reversed(free):
        masks = [mask + more for more in (place, 0) for mask in masks]
    masks = [mask for mask in sorted(masks, key=lambda mask: (mask // base % 4 != 2, -(mask % base))) if mask]
    is_owner = jnp.logical_and(line_z >= 1, line_z <= width_z)
    my_head = (sp % (1 << splits)) * width_z + line_z - 1
    own_at = held + width_z - 1

    @pl.when(is_owner)
    def _():
        settle(qslots.at[pl.ds(0, n_sp - 1)], q_send, q_recv.at[0]).wait_recv()
        qslots[sp] = q_own[...]
        query = jnp.sum(qslots[...], axis=0)
        row_head = lax.broadcasted_iota(jnp.int32, (SUB, DK), 0)
        mine_q = jnp.sum(jnp.where(row_head == my_head, query, 0.0), axis=0, keepdims=True)
        q_wide[...] = jnp.transpose(jnp.broadcast_to(mine_q, (LANES, DK)))

    def follow(line, state):
        settle(gzrecv.at[line], gz_send, gz_recv.at[line]).wait_recv()
        settle(zrecv.at[line, 1], z_send, z_recv.at[line, 1]).wait_recv()
        moved = gzrecv[line, 0:1, 0:1] * state + mm(zrecv[line, 1], state)
        settle(zrecv.at[line, 0], z_send, z_recv.at[line, 0]).wait_recv()
        return moved + zrecv[line, 0].astype(F32)

    def keep_own(state):
        own = maps[own_at]
        return gams[own_at, 0:1, 0:1] * state + mm(own[:, DV:], state) + own[:, :DV]

    for g in range(1, 1 + width_z):

        @pl.when(line_z == g)
        def _(g=g):
            settle(zrecv.at[0, 0], z_send, z_recv.at[0, 0]).wait_recv()
            state = zrecv[0, 0].astype(F32)
            for line in range(1, 4):
                state = keep_own(state) if line == g else follow(line, state)
            final_ref[...] = state

    @pl.when(is_owner)
    def _():
        final = final_ref[...].astype(BF16)
        for j in range(n_sp):
            fstate[j] = final[j * rows_out : (j + 1) * rows_out, :]
        for mask in masks:
            copy_state(mask, my_head).start()
        raw_read = jnp.sum(final.astype(F32) * q_wide[...], axis=0, keepdims=True)
        read = (
            raw_read
            * lax.rsqrt(jnp.mean(raw_read * raw_read, axis=-1, keepdims=True) + norm_eps)
            * gain_ref[...].astype(F32)
        )
        fread[...] = jnp.broadcast_to(read, fread.shape)
        for mask in masks:
            copy_read(mask, my_head).start()
        state_out[my_head] = fstate[sp]
        rrecv[my_head] = fread[...]

    def both_ways(act):
        for owns, number in ((True, -1), (False, 0)):

            @pl.when(is_owner == owns)
            def _(number=number):
                act(number)

    settle(xg.at[pl.ds(0, 2 * n_y - 1)], tok_send, own_recv.at[0]).wait_send()
    settle(sendbuf, map_send, map_recv.at[0, 0]).wait_send()
    settle(gsend, g_send, g_recv.at[0]).wait_send()
    both_ways(
        lambda number: settle(
            qslots.at[pl.ds(0, len(owners) + number)], q_send, q_recv.at[0]
        ).wait_send()
    )

    @pl.when(line_z == 0)
    def _():
        settle(zsend.at[:, 0], z_send, z_recv.at[0, 0]).wait_send()

    for line in range(1, 4):
        number = width_z - 1 if line <= width_z else width_z
        if number:

            @pl.when(line_z == line)
            def _(number=number):
                settle(zsend.at[pl.ds(0, number)], z_send, z_recv.at[0, 0]).wait_send()
                settle(gzsend.at[pl.ds(0, number)], gz_send, gz_recv.at[0]).wait_send()

    def states_in(number):
        if heads + number:
            held_rows = state_out.at[pl.ds(0, heads + number)]
            settle(held_rows, s_send, s_recv.at[0]).wait_recv()
            settle(rrecv.at[pl.ds(0, heads + number)], r_send, r_recv.at[0]).wait_recv()

    both_ways(states_in)
    for h in range(heads):
        read_out[h : h + 1, :] = rrecv[h, 0:1, :]

    @pl.when(is_owner)
    def _():
        settle(fstate.at[pl.ds(0, len(masks))], s_send, s_recv.at[0]).wait_send()
        settle(qslots.at[pl.ds(0, len(masks))], r_send, r_recv.at[0]).wait_send()


def hand_over(state_ref, read_ref, state_out, read_out):
    state_out[...] = state_ref[...]
    read_out[...] = read_ref[...]


def per_device(
    n_sp,
    n_tp,
    tokens,
    w_key,
    w_value,
    w_beta,
    w_decay,
    beta_bias,
    decay_rate,
    forgetting_increment,
    new_query,
    read_gain,
):
    tokens_here, features = tokens.shape
    depth, width = w_key.shape
    heads = width // DK
    parts = tokens_here // CHUNK - 1 + tail_pieces(features)
    rows_out = DK // n_sp
    n_y = n_tp // 2
    total_heads = w_beta.shape[1]
    joins, splits, width_z, copies = tree_shape(n_sp, heads)
    slots = 0
    count = heads
    for _ in range(joins):
        count = max(count // 2, 1)
        slots += count
    vmem = pl.BlockSpec(memory_space=pltpu.VMEM)
    hbm = pl.BlockSpec(memory_space=pl.ANY)
    dma = pltpu.SemaphoreType.DMA
    state, read = pl.pallas_call(
        functools.partial(body, n_sp, n_tp),
        name="delta_state",
        out_shape=(
            pltpu.VMEM((heads, rows_out, DV), BF16),
            pltpu.VMEM((heads, DV), F32),
        ),
        in_specs=[hbm] * 10,
        out_specs=(vmem, vmem),
        scratch_shapes=[
            pltpu.VMEM((depth, width), BF16),
            pltpu.VMEM((depth, width), BF16),
            pltpu.VMEM(w_beta.shape[::-1], BF16),
            pltpu.VMEM(w_decay.shape[::-1], BF16),
            pltpu.VMEM((1, total_heads), F32),
            pltpu.VMEM((1, total_heads), F32),
            pltpu.VMEM(forgetting_increment.shape, F32),
            pltpu.VMEM(new_query.shape, BF16),
            pltpu.VMEM((1, DV), BF16),
            pltpu.VMEM((depth, LANES), BF16),
            pltpu.VMEM((tokens_here, features), BF16),
            pltpu.VMEM((SUB, tokens_here), F32),
            pltpu.VMEM((SUB, DK), F32),
            pltpu.VMEM((n_tp, tokens_here, features), BF16),
            pltpu.VMEM((tokens_here, width), F32),
            pltpu.VMEM((tokens_here, width), F32),
            pltpu.VMEM((tokens_here, LANES), F32),
            pltpu.VMEM((heads, DK, DV + DK), F32),
            pltpu.VMEM((heads, SUB, LANES), F32),
            pltpu.VMEM((slots, 2, DK, DV), BF16),
            pltpu.VMEM((slots, 2, DK, DV), BF16),
            pltpu.VMEM((slots, SUB, LANES), F32),
            pltpu.VMEM((slots, SUB, LANES), F32),
            pltpu.VMEM((width_z, 2, DK, DV), BF16),
            pltpu.VMEM((4, 2, DK, DV), BF16),
            pltpu.VMEM((width_z, SUB, LANES), F32),
            pltpu.VMEM((4, SUB, LANES), F32),
            pltpu.VMEM((n_sp, SUB, DK), F32),
            pltpu.VMEM((DK, LANES), F32),
            pltpu.VMEM((n_sp, rows_out, DV), BF16),
            pltpu.VMEM((DK, DV), F32),
            pltpu.VMEM((SUB, DV), F32),
            pltpu.VMEM((heads, SUB, DV), F32),
            dma((10,)),
            pltpu.SemaphoreType.REGULAR((max(near_rounds(n_sp), 1),)),
            dma((1,)),
            dma((2 * (n_y - 1), parts)),
            dma((1,)),
            dma((slots, 2)),
            dma((joins,)),
            dma((4, 2)),
            dma((4,)),
            dma((1,)),
            dma((1,)),
        ],
        compiler_params=pltpu.CompilerParams(
            collective_id=0, has_side_effects=True, vmem_limit_bytes=63 * 1024 * 1024
        ),
    )(
        tokens,
        w_key,
        w_value,
        w_beta.T,
        w_decay.T,
        beta_bias[None, :],
        decay_rate[None, :],
        forgetting_increment,
        new_query,
        read_gain[None, :],
    )
    return pl.pallas_call(
        hand_over,
        name="hand_over",
        out_shape=(
            jax.ShapeDtypeStruct(state.shape, state.dtype),
            jax.ShapeDtypeStruct(read.shape, read.dtype),
        ),
        in_specs=[vmem, vmem],
        out_specs=(vmem, vmem),
    )(
        pltpu.with_memory_space_constraint(state, pltpu.VMEM),
        pltpu.with_memory_space_constraint(read, pltpu.VMEM),
    )


def solution(mesh):
    return jax.shard_map(
        functools.partial(per_device, mesh.shape["sp"], mesh.shape["tp"]),
        mesh=mesh,
        in_specs=(
            P("sp", "tp"),
            P(None, "tp"),
            P(None, "tp"),
            P(),
            P(),
            P(),
            P(),
            P("tp", "sp"),
            P("tp", "sp"),
            P(),
        ),
        out_specs=(P("tp", "sp", None), P("tp", None)),
        check_vma=False,
    )
```

time: 56 us -> 45.6 us (0.81)
  Pallas kernels: 55.1 us -> 44.8 us
    pallas_call x1, Pallas kernels: 53.8 us -> 44.2 us  [per_device(): pl.pallas_call(functools.partial(body, n_sp, n_tp), name='delta_state', o...]
    pallas_call x1, Pallas kernels: 1.33 us -> 0.61 us  [per_device(): pl.pallas_call(hand_over, name='hand_over', out_shape=(jax.ShapeDtypeStru...]
where the time goes in v1:
time: 45.6 us; the launch traced here: 45.5 us
  Pallas kernels  44.8 us (98%)
  between operations  0.64 us (1%)
    pallas_call x1, Pallas kernels, per_device(): pl.pallas_call(functools.partial(body, n_sp, n_tp), name='delta_state', o...  44.2 us

profile of v1, /device:TPU:0, one launch (start us, length us, event | category | flops | bytes accessed | tf_op | source)
XLA Modules:
  0.0 45.5 jit_solution(18255480722475499601)
XLA Ops:
  0.6 44.2 %delta_state.1 = (bf16[4,16,128]{2,1,0:T(8,128)(2,1)S(1)}, f32[4,128]{1,0:T(4,128)S(1)}) custom-call(bf16[512,1024]{1,0:T(8,128)(2,1)} %x_hbm.1, bf16[4096,512]{1,0:T(8,128)(2,1)} %wk_hbm.1, bf16[4096,512]{1,0:T(8,128)(2,1)} %wv_hbm.1, bf16[16,4096]{1,0:T(8,128)(2,1)} %bitcast.5, bf16[16,4096]{1,0:T(8,128)(2,1)} %bitcast.6, f32[1,16]{1,0:T(1,128)} %bitcast.7, ...), custom_call_target="tpu_custom_call" | custom-call | tf_op jit(solution)/shard_map/delta_state/pallas_call | solution.py:830
  44.9 0.6 %hand_over.1 = (bf16[4,16,128]{2,1,0:T(8,128)(2,1)}, f32[4,128]{1,0:T(4,128)}) custom-call(bf16[4,16,128]{2,1,0:T(8,128)(2,1)S(1)} %get-tuple-element.4.state_ref, f32[4,128]{1,0:T(4,128)S(1)} %get-tuple-element.5.read_ref), custom_call_target="tpu_custom_call" | custom-call | tf_op jit(solution)/shard_map/hand_over/pallas_call | solution.py:900

commit v2 on v1

--- a/solution.py
+++ b/solution.py
@@ -33,7 +33,7 @@
 
 
 def near_rounds(n_sp):
-    return 2 if n_sp == 8 else 0
+    return 3 if n_sp == 8 else 0
 
 
 def tree_shape(n_sp, heads):
@@ -93,8 +93,9 @@
     q_wide,
     fstate,
     final_ref,
-    fread,
-    rrecv,
+    srecv,
+    late_out,
+    late_in,
     wsem,
     ready,
     own_recv,
@@ -105,7 +106,7 @@
     z_recv,
     gz_recv,
     s_recv,
-    r_recv,
+    l_recv,
 ):
     sp = lax.axis_index("sp")
     tp = lax.axis_index("tp")
@@ -126,7 +127,7 @@
     base = 1 << joins
     line_z = sp // base
 
-    (map_send, z_send, s_send, r_send, tok_send, q_send, g_send, gz_send) = (
+    (map_send, z_send, s_send, l_send, tok_send, q_send, g_send, gz_send) = (
         wsem.at[pl.ds(place, 1)] for place in range(8)
     )
     barrier = pltpu.get_barrier_semaphore()
@@ -327,11 +328,15 @@
     if rounds:
         pl.semaphore_wait(ready.at[rounds - 1], near_count)
 
-    def owner_of(h, copy):
-        return (1 + h % width_z) * base + h // width_z + (copy << splits)
+    lanes_of = 1 << splits
+
+    def reader_of(h, copy):
+        if h < heads:
+            return (1 + h % width_z) * base + h // width_z + (copy << splits)
+        return 3 * base + h - heads + (copy << splits)
 
     def copy_query(h, copy):
-        owner = owner_of(h, copy)
+        owner = reader_of(h, copy)
         return pltpu.make_async_remote_copy(
             src_ref=q_own,
             dst_ref=qslots.at[sp],
@@ -341,10 +346,10 @@
             device_id_type=MESH,
         )
 
-    owners = [(h, copy) for h in range(heads) for copy in range(copies)]
-    for h, copy in owners:
-
-        @pl.when(sp != owner_of(h, copy))
+    readers = [(h, copy) for h in range(heads + lanes_of) for copy in range(copies)]
+    for h, copy in readers:
+
+        @pl.when(sp != reader_of(h, copy))
         def _(h=h, copy=copy):
             copy_query(h, copy).start()
 
@@ -502,9 +507,8 @@
             far_take(last + 1)
             end_project(far, 0, 2)
             far_take(last + 2)
-            end_project(far, 2, 1)
             far_take(last + 3)
-            end_project(far, 3, 1)
+            end_project(far, 2, 2)
 
         @pl.when(core == 0)
         def _():
@@ -649,7 +653,7 @@
             if top:
                 zsend[j, 0] = joined.astype(BF16)
 
-                @pl.when(line_z != goal(j))
+                @pl.when(jnp.logical_and(line_z != goal(j), line_z < 3))
                 def _(j=j):
                     copy_up(j, 0).start()
 
@@ -661,20 +665,20 @@
         target = flip(mask)
         return pltpu.make_async_remote_copy(
             src_ref=fstate.at[target],
-            dst_ref=state_out.at[h],
+            dst_ref=srecv.at[h],
             send_sem=s_send.at[0],
             recv_sem=s_recv.at[0],
             device_id={"sp": target},
             device_id_type=MESH,
         )
 
-    def copy_read(mask, h):
+    def copy_late(mask):
         target = flip(mask)
         return pltpu.make_async_remote_copy(
-            src_ref=fread,
-            dst_ref=rrecv.at[h],
-            send_sem=r_send.at[0],
-            recv_sem=r_recv.at[0],
+            src_ref=late_out.at[target],
+            dst_ref=late_in.at[sp % lanes_of],
+            send_sem=l_send.at[0],
+            recv_sem=l_recv.at[0],
             device_id={"sp": target},
             device_id_type=MESH,
         )
@@ -695,79 +699,113 @@
         masks = [mask + more for more in (place, 0) for mask in masks]
     masks = [mask for mask in sorted(masks, key=lambda mask: (mask // base % 4 != 2, -(mask % base))) if mask]
     is_owner = jnp.logical_and(line_z >= 1, line_z <= width_z)
-    my_head = (sp % (1 << splits)) * width_z + line_z - 1
+    is_last = line_z == 3
+    reads_query = jnp.logical_or(is_owner, is_last)
+    my_lane = sp % lanes_of
+    my_head = my_lane * width_z + line_z - 1
     own_at = held + width_z - 1
-
-    @pl.when(is_owner)
+    space = srecv.shape[1] - SUB
+    row_head = lax.broadcasted_iota(jnp.int32, (SUB, DK), 0)
+
+    @pl.when(reads_query)
     def _():
         settle(qslots.at[pl.ds(0, n_sp - 1)], q_send, q_recv.at[0]).wait_recv()
         qslots[sp] = q_own[...]
+
+    @pl.when(is_last)
+    def _():
         query = jnp.sum(qslots[...], axis=0)
-        row_head = lax.broadcasted_iota(jnp.int32, (SUB, DK), 0)
+        for i in range(width_z):
+            part = maps[held + i, :, :DV]
+            reads = mm(query, part)
+            wanted = row_head == my_lane * width_z + i
+            line_read = jnp.sum(jnp.where(wanted, reads, 0.0), axis=0, keepdims=True)
+            for j in range(n_sp):
+                late_out[j, i * space : i * space + rows_out, :] = part[
+                    j * rows_out : (j + 1) * rows_out, :
+                ]
+                late_out[j, width_z * space + i : width_z * space + i + 1, :] = line_read
+        for mask in masks:
+            copy_late(mask).start()
+        late_in[my_lane] = late_out[sp]
+
+    @pl.when(is_owner)
+    def _():
+        query = jnp.sum(qslots[...], axis=0)
         mine_q = jnp.sum(jnp.where(row_head == my_head, query, 0.0), axis=0, keepdims=True)
         q_wide[...] = jnp.transpose(jnp.broadcast_to(mine_q, (LANES, DK)))
 
+    def landed(line, part):
+        settle(zrecv.at[line, part], z_send, z_recv.at[line, part]).wait_recv()
+        return zrecv[line, part]
+
+    def landed_gamma(line):
+        settle(gzrecv.at[line], gz_send, gz_recv.at[line]).wait_recv()
+        return gzrecv[line, 0:1, 0:1]
+
     def follow(line, state):
-        settle(gzrecv.at[line], gz_send, gz_recv.at[line]).wait_recv()
-        settle(zrecv.at[line, 1], z_send, z_recv.at[line, 1]).wait_recv()
-        moved = gzrecv[line, 0:1, 0:1] * state + mm(zrecv[line, 1], state)
-        settle(zrecv.at[line, 0], z_send, z_recv.at[line, 0]).wait_recv()
-        return moved + zrecv[line, 0].astype(F32)
-
-    def keep_own(state):
-        own = maps[own_at]
-        return gams[own_at, 0:1, 0:1] * state + mm(own[:, DV:], state) + own[:, :DV]
+        gamma = landed_gamma(line)
+        moved = gamma * state + mm(landed(line, 1), state)
+        return moved + landed(line, 0).astype(F32) if line < 3 else moved
 
     for g in range(1, 1 + width_z):
 
         @pl.when(line_z == g)
         def _(g=g):
-            settle(zrecv.at[0, 0], z_send, z_recv.at[0, 0]).wait_recv()
-            state = zrecv[0, 0].astype(F32)
-            for line in range(1, 4):
-                state = keep_own(state) if line == g else follow(line, state)
-            final_ref[...] = state
+            own = maps[own_at]
+            own_g = gams[own_at, 0:1, 0:1]
+            if g == 1:
+                gamma = landed_gamma(2)
+                erase = landed(2, 1).astype(F32)
+                both = gamma * own + mm(erase, own)
+                both_b = both[:, :DV] + landed(2, 0).astype(F32)
+                both_n = both[:, DV:] + own_g * erase
+                first = landed(0, 0).astype(F32)
+                state = (gamma * own_g) * first + mm(both_n, first) + both_b
+            else:
+                state = follow(1, landed(0, 0).astype(F32))
+                state = own_g * state + mm(own[:, DV:], state) + own[:, :DV]
+            final_ref[...] = follow(3, state)
 
     @pl.when(is_owner)
     def _():
-        final = final_ref[...].astype(BF16)
+        final = final_ref[...]
+        raw_read = jnp.sum(final * q_wide[...], axis=0, keepdims=True)
         for j in range(n_sp):
-            fstate[j] = final[j * rows_out : (j + 1) * rows_out, :]
+            fstate[j, 0:rows_out, :] = final[j * rows_out : (j + 1) * rows_out, :]
+            fstate[j, space : space + 1, :] = raw_read
         for mask in masks:
             copy_state(mask, my_head).start()
-        raw_read = jnp.sum(final.astype(F32) * q_wide[...], axis=0, keepdims=True)
-        read = (
-            raw_read
-            * lax.rsqrt(jnp.mean(raw_read * raw_read, axis=-1, keepdims=True) + norm_eps)
-            * gain_ref[...].astype(F32)
-        )
-        fread[...] = jnp.broadcast_to(read, fread.shape)
-        for mask in masks:
-            copy_read(mask, my_head).start()
-        state_out[my_head] = fstate[sp]
-        rrecv[my_head] = fread[...]
-
-    def both_ways(act):
-        for owns, number in ((True, -1), (False, 0)):
-
-            @pl.when(is_owner == owns)
-            def _(number=number):
-                act(number)
+        srecv[my_head] = fstate[sp]
 
     settle(xg.at[pl.ds(0, 2 * n_y - 1)], tok_send, own_recv.at[0]).wait_send()
     settle(sendbuf, map_send, map_recv.at[0, 0]).wait_send()
     settle(gsend, g_send, g_recv.at[0]).wait_send()
-    both_ways(
-        lambda number: settle(
-            qslots.at[pl.ds(0, len(owners) + number)], q_send, q_recv.at[0]
-        ).wait_send()
-    )
+
+    def depending(test, act, no, yes):
+        for value, number in ((False, no), (True, yes)):
+
+            @pl.when(test == value)
+            def _(number=number):
+                if number:
+                    act(number)
+
+    def queries_out(number):
+        settle(qslots.at[pl.ds(0, number)], q_send, q_recv.at[0]).wait_send()
+
+    depending(reads_query, queries_out, len(readers), len(readers) - 1)
 
     @pl.when(line_z == 0)
     def _():
         settle(zsend.at[:, 0], z_send, z_recv.at[0, 0]).wait_send()
 
-    for line in range(1, 4):
+    @pl.when(is_last)
+    def _():
+        settle(zsend.at[:, 1], z_send, z_recv.at[0, 0]).wait_send()
+        settle(gzsend, gz_send, gz_recv.at[0]).wait_send()
+        settle(late_out.at[pl.ds(0, len(masks))], l_send, l_recv.at[0]).wait_send()
+
+    for line in range(1, 3):
         number = width_z - 1 if line <= width_z else width_z
         if number:
 
@@ -776,20 +814,29 @@
                 settle(zsend.at[pl.ds(0, number)], z_send, z_recv.at[0, 0]).wait_send()
                 settle(gzsend.at[pl.ds(0, number)], gz_send, gz_recv.at[0]).wait_send()
 
+    def late_ones(number):
+        settle(late_in.at[pl.ds(0, number)], l_send, l_recv.at[0]).wait_recv()
+
     def states_in(number):
-        if heads + number:
-            held_rows = state_out.at[pl.ds(0, heads + number)]
-            settle(held_rows, s_send, s_recv.at[0]).wait_recv()
-            settle(rrecv.at[pl.ds(0, heads + number)], r_send, r_recv.at[0]).wait_recv()
-
-    both_ways(states_in)
+        settle(srecv.at[pl.ds(0, number)], s_send, s_recv.at[0]).wait_recv()
+
+    depending(is_last, late_ones, lanes_of, lanes_of - 1)
+    gain = gain_ref[...].astype(F32)
+    depending(is_owner, states_in, heads, heads - 1)
     for h in range(heads):
-        read_out[h : h + 1, :] = rrecv[h, 0:1, :]
+        lane, i = h // width_z, h % width_z
+        state_out[h] = (
+            srecv[h, 0:rows_out, :] + late_in[lane, i * space : i * space + rows_out, :]
+        ).astype(BF16)
+        at = width_z * space + i
+        raw = srecv[h, space : space + 1, :] + late_in[lane, at : at + 1, :]
+        read_out[h : h + 1, :] = (
+            raw * lax.rsqrt(jnp.mean(raw * raw, axis=-1, keepdims=True) + norm_eps) * gain
+        )
 
     @pl.when(is_owner)
     def _():
         settle(fstate.at[pl.ds(0, len(masks))], s_send, s_recv.at[0]).wait_send()
-        settle(qslots.at[pl.ds(0, len(masks))], r_send, r_recv.at[0]).wait_send()
 
 
 def hand_over(state_ref, read_ref, state_out, read_out):
@@ -819,6 +866,7 @@
     n_y = n_tp // 2
     total_heads = w_beta.shape[1]
     joins, splits, width_z, copies = tree_shape(n_sp, heads)
+    space = -(-rows_out // SUB) * SUB
     slots = 0
     count = heads
     for _ in range(joins):
@@ -866,10 +914,11 @@
             pltpu.VMEM((4, SUB, LANES), F32),
             pltpu.VMEM((n_sp, SUB, DK), F32),
             pltpu.VMEM((DK, LANES), F32),
-            pltpu.VMEM((n_sp, rows_out, DV), BF16),
+            pltpu.VMEM((n_sp, space + SUB, DV), F32),
             pltpu.VMEM((DK, DV), F32),
-            pltpu.VMEM((SUB, DV), F32),
-            pltpu.VMEM((heads, SUB, DV), F32),
+            pltpu.VMEM((heads, space + SUB, DV), F32),
+            pltpu.VMEM((n_sp, width_z * space + SUB, DV), F32),
+            pltpu.VMEM((1 << splits, width_z * space + SUB, DV), F32),
             dma((10,)),
             pltpu.SemaphoreType.REGULAR((max(near_rounds(n_sp), 1),)),
             dma((1,)),

time: 45.6 us -> 45.6 us (level)
  no operation moved by 1% of the time
where the time goes in v2:
time: 45.6 us; the launch traced here: 45.5 us
  Pallas kernels  44.8 us (98%)
  between operations  0.64 us (1%)
    pallas_call x1, Pallas kernels, per_device(): pl.pallas_call(functools.partial(body, n_sp, n_tp), name='delta_state', o...  44.2 us

profile of v2, /device:TPU:0, one launch (start us, length us, event | category | flops | bytes accessed | tf_op | source)
XLA Modules:
  0.0 45.5 jit_solution(8336269272622030538)
XLA Ops:
  0.6 44.2 %delta_state.1 = (bf16[4,16,128]{2,1,0:T(8,128)(2,1)S(1)}, f32[4,128]{1,0:T(4,128)S(1)}) custom-call(bf16[512,1024]{1,0:T(8,128)(2,1)} %x_hbm.1, bf16[4096,512]{1,0:T(8,128)(2,1)} %wk_hbm.1, bf16[4096,512]{1,0:T(8,128)(2,1)} %wv_hbm.1, bf16[16,4096]{1,0:T(8,128)(2,1)} %bitcast.5, bf16[16,4096]{1,0:T(8,128)(2,1)} %bitcast.6, f32[1,16]{1,0:T(1,128)} %bitcast.7, ...), custom_call_target="tpu_custom_call" | custom-call | tf_op jit(solution)/shard_map/delta_state/pallas_call | solution.py:878
  44.9 0.6 %hand_over.1 = (bf16[4,16,128]{2,1,0:T(8,128)(2,1)}, f32[4,128]{1,0:T(4,128)}) custom-call(bf16[4,16,128]{2,1,0:T(8,128)(2,1)S(1)} %get-tuple-element.4.state_ref, f32[4,128]{1,0:T(4,128)S(1)} %get-tuple-element.5.read_ref), custom_call_target="tpu_custom_call" | custom-call | tf_op jit(solution)/shard_map/hand_over/pallas_call | solution.py:949

commit v3 on v2

--- a/solution.py
+++ b/solution.py
@@ -12,6 +12,7 @@
 CHUNK = 128
 LANES = 128
 SUB = 8
+TILE = 16
 norm_eps = 1e-06
 MESH = pl.DeviceIdType.MESH
 F32 = jnp.float32
@@ -81,6 +82,7 @@
     accg,
     maps,
     gams,
+    pair,
     sendbuf,
     recvbuf,
     gsend,
@@ -603,15 +605,32 @@
         copy_gamma(level, offset, half, partner).start()
         if level == 0:
             advance(end_rows, end_terms, first_out, end_found)
+        top = level == joins - 1
         for j in range(half):
-            slot = offset + j
-            sendbuf[slot, 1] = maps[send_at + j, :, DV:].astype(BF16)
-            copy_map(slot, 1, partner).start()
-            sendbuf[slot, 0] = maps[send_at + j, :, :DV].astype(BF16)
-            copy_map(slot, 0, partner).start()
+            for part in (1, 0):
+                cols = pl.ds(part * DV, DV)
+                sendbuf[offset + j, part] = maps[send_at + j, :, cols].astype(BF16)
+        usual = [(j, part) for j in range(half) for part in (1, 0)]
+        erase_first = [(j, part) for part in (1, 0) for j in range(half)]
+
+        def start_all(order):
+            for j, part in order:
+                copy_map(offset + j, part, partner).start()
+
+        if top and half > 1:
+
+            @pl.when(line_z < 3)
+            def _():
+                start_all(usual)
+
+            @pl.when(line_z == 3)
+            def _():
+                start_all(erase_first)
+
+        else:
+            start_all(usual)
         if level == 0 and split:
             advance(end_rows, end_terms, range(half, heads))
-        top = level == joins - 1
         copy_gamma(level, offset, half, partner).wait_recv()
         if top:
             for j in range(half):
@@ -621,42 +640,55 @@
                 def _(j=j):
                     copy_up_gamma(j).start()
 
-        for j in range(half):
-            slot = offset + j
-            own = maps[keep_at + j]
+        def sides(j, part):
+            own = maps[keep_at + j, :, pl.ds(part * DV, DV)]
             if not split:
                 own = own.astype(BF16).astype(F32)
-            own_g = gams[keep_at + j]
-            got_g = grecv[slot]
+            got = recvbuf[offset + j, part].astype(F32)
+            return jnp.where(later, own, got), jnp.where(later, got, own)
+
+        def join(j, part):
+            own_g, got_g = gams[keep_at + j], grecv[offset + j]
+            copy_map(offset + j, part, partner).wait_recv()
             left_g = jnp.where(later, own_g, got_g)[0:1, 0:1]
             right_g = jnp.where(later, got_g, own_g)[0:1, 0:1]
-            gams[keep_at + j] = own_g * got_g
-            copy_map(slot, 1, partner).wait_recv()
-            got = recvbuf[slot, 1].astype(F32)
-            left = jnp.where(later, own[:, DV:], got)
-            right = jnp.where(later, got, own[:, DV:])
-            joined = left_g * right + mm(left, right) + right_g * left
-            maps[keep_at + j, :, DV:] = joined
-            if top:
-                zsend[j, 1] = joined.astype(BF16)
-
-                @pl.when(jnp.logical_and(line_z != goal(j), line_z > 0))
-                def _(j=j):
-                    copy_up(j, 1).start()
-
-            copy_map(slot, 0, partner).wait_recv()
-            got = recvbuf[slot, 0].astype(F32)
-            left_b = jnp.where(later, own[:, :DV], got)
-            right_b = jnp.where(later, got, own[:, :DV])
-            joined = left_g * right_b + mm(left, right_b) + left_b
-            maps[keep_at + j, :, :DV] = joined
-            if top:
-                zsend[j, 0] = joined.astype(BF16)
-
-                @pl.when(jnp.logical_and(line_z != goal(j), line_z < 3))
-                def _(j=j):
-                    copy_up(j, 0).start()
-
+            left, right = sides(j, part)
+            if part:
+                return left_g * right + mm(left, right) + right_g * left
+            return left_g * right + mm(sides(j, 1)[0], right) + left
+
+        def join_top(j, part):
+            joined = join(j, part)
+            pair[j, :, pl.ds(part * DV, DV)] = joined
+            zsend[j, part] = joined.astype(BF16)
+            sends = line_z > 0 if part else line_z < 3
+
+            @pl.when(jnp.logical_and(line_z != goal(j), sends))
+            def _():
+                copy_up(j, part).start()
+
+        if not top:
+            for j in range(half):
+                both = [join(j, part) for part in (0, 1)]
+                maps[keep_at + j] = jnp.concatenate(both, axis=1)
+                gams[keep_at + j] = gams[keep_at + j] * grecv[offset + j]
+        elif half == 2:
+            join_top(0, 1)
+
+            @pl.when(line_z < 3)
+            def _():
+                join_top(0, 0)
+
+            join_top(1, 1)
+
+            @pl.when(line_z == 3)
+            def _():
+                join_top(0, 0)
+
+            join_top(1, 0)
+        else:
+            for j, part in usual:
+                join_top(j, part)
         offset += half
         count = half
         held = keep_at
@@ -703,8 +735,19 @@
     reads_query = jnp.logical_or(is_owner, is_last)
     my_lane = sp % lanes_of
     my_head = my_lane * width_z + line_z - 1
-    own_at = held + width_z - 1
-    space = srecv.shape[1] - SUB
+    own_at = width_z - 1
+    space = srecv.shape[1] - TILE
+
+    def three_rows(row):
+        high = row.astype(BF16)
+        rest = row - high.astype(F32)
+        middle = rest.astype(BF16)
+        return high, middle, (rest - middle.astype(F32)).astype(BF16)
+
+    def one_row(ref, lead_at, at):
+        found = ref[lead_at, at : at + 8, :].astype(F32)
+        return found[0:1] + found[1:2] + found[2:3]
+
     row_head = lax.broadcasted_iota(jnp.int32, (SUB, DK), 0)
 
     @pl.when(reads_query)
@@ -716,16 +759,19 @@
     def _():
         query = jnp.sum(qslots[...], axis=0)
         for i in range(width_z):
-            part = maps[held + i, :, :DV]
+            part = pair[i, :, :DV]
             reads = mm(query, part)
             wanted = row_head == my_lane * width_z + i
             line_read = jnp.sum(jnp.where(wanted, reads, 0.0), axis=0, keepdims=True)
+            at = width_z * space + i * SUB
+            rounded = part.astype(BF16)
+            block = jnp.concatenate([*three_rows(line_read), jnp.zeros((SUB - 3, DV), BF16)], axis=0)
             for j in range(n_sp):
-                late_out[j, i * space : i * space + rows_out, :] = part[
+                late_out[j, i * space : i * space + rows_out, :] = rounded[
                     j * rows_out : (j + 1) * rows_out, :
                 ]
-                late_out[j, width_z * space + i : width_z * space + i + 1, :] = line_read
-        for mask in masks:
+                late_out[j, at : at + SUB, :] = block
+        for mask in sorted(masks, reverse=True):
             copy_late(mask).start()
         late_in[my_lane] = late_out[sp]
 
@@ -752,8 +798,8 @@
 
         @pl.when(line_z == g)
         def _(g=g):
-            own = maps[own_at]
-            own_g = gams[own_at, 0:1, 0:1]
+            own = pair[own_at]
+            own_g = gzsend[own_at, 0:1, 0:1]
             if g == 1:
                 gamma = landed_gamma(2)
                 erase = landed(2, 1).astype(F32)
@@ -771,9 +817,11 @@
     def _():
         final = final_ref[...]
         raw_read = jnp.sum(final * q_wide[...], axis=0, keepdims=True)
+        rounded = final.astype(BF16)
+        block = jnp.concatenate([*three_rows(raw_read), jnp.zeros((SUB - 3, DV), BF16)], axis=0)
         for j in range(n_sp):
-            fstate[j, 0:rows_out, :] = final[j * rows_out : (j + 1) * rows_out, :]
-            fstate[j, space : space + 1, :] = raw_read
+            fstate[j, 0:rows_out, :] = rounded[j * rows_out : (j + 1) * rows_out, :]
+            fstate[j, space : space + SUB, :] = block
         for mask in masks:
             copy_state(mask, my_head).start()
         srecv[my_head] = fstate[sp]
@@ -826,10 +874,10 @@
     for h in range(heads):
         lane, i = h // width_z, h % width_z
         state_out[h] = (
-            srecv[h, 0:rows_out, :] + late_in[lane, i * space : i * space + rows_out, :]
+            srecv[h, 0:rows_out, :].astype(F32)
+            + late_in[lane, i * space : i * space + rows_out, :].astype(F32)
         ).astype(BF16)
-        at = width_z * space + i
-        raw = srecv[h, space : space + 1, :] + late_in[lane, at : at + 1, :]
+        raw = one_row(srecv, h, space) + one_row(late_in, lane, width_z * space + i * SUB)
         read_out[h : h + 1, :] = (
             raw * lax.rsqrt(jnp.mean(raw * raw, axis=-1, keepdims=True) + norm_eps) * gain
         )
@@ -866,7 +914,7 @@
     n_y = n_tp // 2
     total_heads = w_beta.shape[1]
     joins, splits, width_z, copies = tree_shape(n_sp, heads)
-    space = -(-rows_out // SUB) * SUB
+    space = -(-rows_out // TILE) * TILE
     slots = 0
     count = heads
     for _ in range(joins):
@@ -904,6 +952,7 @@
             pltpu.VMEM((tokens_here, LANES), F32),
             pltpu.VMEM((heads, DK, DV + DK), F32),
             pltpu.VMEM((heads, SUB, LANES), F32),
+            pltpu.VMEM((width_z, DK, DV + DK), F32),
             pltpu.VMEM((slots, 2, DK, DV), BF16),
             pltpu.VMEM((slots, 2, DK, DV), BF16),
             pltpu.VMEM((slots, SUB, LANES), F32),
@@ -914,11 +963,11 @@
             pltpu.VMEM((4, SUB, LANES), F32),
             pltpu.VMEM((n_sp, SUB, DK), F32),
             pltpu.VMEM((DK, LANES), F32),
-            pltpu.VMEM((n_sp, space + SUB, DV), F32),
+            pltpu.VMEM((n_sp, space + TILE, DV), BF16),
             pltpu.VMEM((DK, DV), F32),
-            pltpu.VMEM((heads, space + SUB, DV), F32),
-            pltpu.VMEM((n_sp, width_z * space + SUB, DV), F32),
-            pltpu.VMEM((1 << splits, width_z * space + SUB, DV), F32),
+            pltpu.VMEM((heads, space + TILE, DV), BF16),
+            pltpu.VMEM((n_sp, width_z * space + TILE, DV), BF16),
+            pltpu.VMEM((1 << splits, width_z * space + TILE, DV), BF16),
             dma((10,)),
             pltpu.SemaphoreType.REGULAR((max(near_rounds(n_sp), 1),)),
             dma((1,)),

time: 45.6 us -> 44.6 us (0.978)
  Pallas kernels: 44.8 us -> 43.8 us
    pallas_call x1, Pallas kernels: 44.2 us -> 43.2 us  [per_device(): pl.pallas_call(functools.partial(body, n_sp, n_tp), name='delta_state', o...]
where the time goes in v3:
time: 44.6 us; the launch traced here: 44.4 us
  Pallas kernels  43.8 us (98%)
  between operations  0.64 us (1%)
    pallas_call x1, Pallas kernels, per_device(): pl.pallas_call(functools.partial(body, n_sp, n_tp), name='delta_state', o...  43.2 us

profile of v3, /device:TPU:0, one launch (start us, length us, event | category | flops | bytes accessed | tf_op | source)
XLA Modules:
  0.0 44.4 jit_solution(11815017379910633764)
XLA Ops:
  0.6 43.2 %delta_state.1 = (bf16[4,16,128]{2,1,0:T(8,128)(2,1)S(1)}, f32[4,128]{1,0:T(4,128)S(1)}) custom-call(bf16[512,1024]{1,0:T(8,128)(2,1)} %x_hbm.1, bf16[4096,512]{1,0:T(8,128)(2,1)} %wk_hbm.1, bf16[4096,512]{1,0:T(8,128)(2,1)} %wv_hbm.1, bf16[16,4096]{1,0:T(8,128)(2,1)} %bitcast.5, bf16[16,4096]{1,0:T(8,128)(2,1)} %bitcast.6, f32[1,16]{1,0:T(1,128)} %bitcast.7, ...), custom_call_target="tpu_custom_call" | custom-call | tf_op jit(solution)/shard_map/delta_state/pallas_call | solution.py:926
  43.8 0.6 %hand_over.1 = (bf16[4,16,128]{2,1,0:T(8,128)(2,1)}, f32[4,128]{1,0:T(4,128)}) custom-call(bf16[4,16,128]{2,1,0:T(8,128)(2,1)S(1)} %get-tuple-element.4.state_ref, f32[4,128]{1,0:T(4,128)S(1)} %get-tuple-element.5.read_ref), custom_call_target="tpu_custom_call" | custom-call | tf_op jit(solution)/shard_map/hand_over/pallas_call | solution.py:998
